TPU v7x, 256 devices: a whole 4x4x8 slice. The times are simulated.
256 devices in a mesh: sp: 64 (over z, y, core), tp: 4 (over x).
Axes of the slice: x: 4, y: 4, z: 8, core: 2. Of those that a mesh axis runs over, the one named last changes fastest.
Arguments:
- conv_input: bfloat16 [16384, 2048], P('sp', 'tp'), may hold values from -6 to 6
- gate_branch: bfloat16 [16384, 2048], P('sp', 'tp'), may hold values from -6 to 6
- conv_taps: float32 [4, 2048], P(None, 'tp'), may hold values from -3 to 3
- narrow_maps: bfloat16 [2, 8, 128, 128], P(None, 'tp'), may hold values from -0.5 to 0.5
- wide_maps: bfloat16 [2, 4, 256, 256], P(None, 'tp'), may hold values from -0.375 to 0.375
- decay_param: float32 [2048], P('tp'), may hold values from 4.5 to 20
- decay_shift: float32 [16384, 2048], P('sp', 'tp'), may hold values from -0.75 to 0
- mixer_out: bfloat16 [2048, 2048], P('tp'), may hold values from -0.125 to 0.125
- stream: bfloat16 [16384, 2048], P(('sp', 'tp')), may hold values from -6 to 6
- norm_gain: float32 [2048], replicated, may hold values from 0.1 to 1.9
- routes: int32 [16384, 4], P('sp'), may hold values from 0 to 63, all different within a row; in each aligned block of 64 rows (0 to 63, 64 to 127, ...) at most 8 rows name the same one
- route_weights: float32 [16384, 4], P('sp'), may hold values from 0.05 to 0.5
- expert_gate: bfloat16 [64, 2048, 2048], P('sp', None, 'tp'), may hold values from -1 to 1
- expert_up: bfloat16 [64, 2048, 2048], P('sp', None, 'tp'), may hold values from -1 to 1
- expert_down: bfloat16 [64, 2048, 2048], P('sp', 'tp'), may hold values from -0.015625 to 0.015625
Outputs:
- layer_out: bfloat16 [16384, 2048], P(('sp', 'tp'))
Inputs may be any that keep to these rules, and one draw needn't show every extreme that they name: `routes`: each row names 4 different experts. In each aligned block of 64 rows no expert is named more than 8 times, and in every draw some expert is named exactly 8 times in some block.
All inputs are finite; a program needn't handle non-finite values.
Results may differ from a plain program's by a relative error of at most 0.015.
Values may be sent and summed in bfloat16 or wider, within the bound.
A program may use at most 128 MiB of HBM per device.

v0:
```python
import jax
import jax.numpy as jnp
from jax import lax
from jax.sharding import PartitionSpec as P

NORM_EPSILON = 1e-06
CLAMP_LIMIT = 7.0
GATE_SLOPE = 1.702
DECAY_SCALE = 8.0


def shifted(block, axis, distance):
    devices = range(lax.axis_size(axis))
    route = [(i - distance, i) for i in devices if i - distance in devices]
    return lax.ppermute(block, axis, route)


def from_everyone(x, axis):
    copies = jnp.broadcast_to(x, (lax.axis_size(axis), *x.shape))
    return lax.all_to_all(copies, axis, split_axis=0, concat_axis=0, tiled=True)


def gathered_once(x, axis):
    leaves = jax.tree.leaves(x)
    turns = sorted(range(len(leaves)), key=lambda k: -leaves[k].size)
    width = (1, *leaves[turns[0]].shape)[-1]
    lines = [
        jnp.pad(leaves[k].reshape(-1), (0, -leaves[k].size % width)).reshape(-1, width)
        for k in turns
    ]
    both, at, found = (from_everyone(jnp.concatenate(lines), axis), 0, {})
    for k, line in zip(turns, lines):
        share = both[:, at : at + len(line)].reshape(len(both), -1)
        found[k] = share[:, : leaves[k].size].reshape(-1, *leaves[k].shape)
        at += len(line)
    numbers = iter(range(len(leaves)))
    return jax.tree.map(lambda _: found[next(numbers)], x)


def combined_pairwise(pieces, combine):
    while len(jax.tree.leaves(pieces)[0]) > 1:
        pieces = jax.vmap(combine)(
            *(jax.tree.map(lambda part: part[side::2], pieces) for side in (0, 1))
        )
    return jax.tree.map(lambda part: part[0], pieces)


def entering(x, axis, combine, identity):
    length, mine = (lax.axis_size(axis), lax.axis_index(axis))
    passed = jnp.arange(length) < mine

    def kept(part, zero, own):
        part = jnp.where(
            passed.reshape(-1, *(1 for _ in own.shape)), part, jnp.asarray(zero, own.dtype)
        )
        return part

    pieces = gathered_once(x, axis)
    return combined_pairwise(jax.tree.map(kept, pieces, identity, x), combine)


def cut_along(x, dim, length):
    lengths = x.shape
    blocks = x.reshape(*lengths[:dim], length, lengths[dim] // length, *lengths[dim + 1 :])
    return jnp.moveaxis(blocks, dim, 0)


def sum_at_owner(x, axis, dim):
    length = lax.axis_size(axis)
    blocks = lax.all_to_all(cut_along(x, dim, length), axis, 0, 0, tiled=True)
    return jnp.sum(blocks.astype(jnp.float32), axis=0)


def combine_steps(earlier, later):
    return (earlier[0] * later[0], later[0] * earlier[1] + later[1])


def head_maps(convolved, narrow_maps, wide_maps):
    seq_rows = convolved.shape[0]
    wide_count = wide_maps.shape[1]
    wide_size = wide_maps.shape[2]
    narrow_size = narrow_maps.shape[2]
    segments = convolved.reshape(seq_rows, wide_count, 2 * narrow_size + wide_size)
    narrow = segments[:, :, : 2 * narrow_size].reshape(seq_rows, 2 * wide_count, narrow_size)
    wide_part = segments[:, :, 2 * narrow_size :]
    narrow_pre = jnp.einsum(
        "rhi,mhio->mrho", narrow, narrow_maps, preferred_element_type=jnp.float32
    )
    wide_pre = jnp.einsum(
        "rhi,mhio->mrho", wide_part, wide_maps, preferred_element_type=jnp.float32
    )
    narrow_pre = narrow_pre.reshape(2, seq_rows, wide_count, 2 * narrow_size)
    return jnp.concatenate([narrow_pre, wide_pre], axis=3).reshape(2, seq_rows, convolved.shape[1])


def clamp_units(gate_pre, up_pre):
    clamped = jnp.minimum(gate_pre, CLAMP_LIMIT)
    upper = jnp.clip(up_pre, -CLAMP_LIMIT, CLAMP_LIMIT)
    return (upper + 1.0) * clamped * jax.nn.sigmoid(GATE_SLOPE * clamped)


def slot_ranks(flat_routes, expert_total):
    onehot = (
        flat_routes[:, :, None] == jnp.arange(expert_total, dtype=jnp.int32)[None, None, :]
    ).astype(jnp.int32)
    return jnp.sum(jnp.cumsum(onehot, axis=1) * onehot, axis=2) - 1


def take_rows(source_rows, slot_source):
    filled = slot_source >= 0
    picked = source_rows[jnp.maximum(slot_source, 0)]
    return jnp.where(filled[:, None], picked, jnp.zeros_like(picked))


def expert_work(arrived, expert_gate, expert_up, expert_down):
    local_experts = expert_gate.shape[0]
    buffer_shape = arrived.shape
    grouped = arrived.reshape(
        buffer_shape[0] // local_experts,
        local_experts,
        buffer_shape[1] * buffer_shape[2],
        buffer_shape[3],
    )
    gate_pre = jnp.einsum(
        "sxcd,xdf->sxcf", grouped, expert_gate, preferred_element_type=jnp.float32
    )
    up_pre = jnp.einsum("sxcd,xdf->sxcf", grouped, expert_up, preferred_element_type=jnp.float32)
    activation = clamp_units(gate_pre, up_pre).astype(jnp.bfloat16)
    partial_value = jnp.einsum(
        "sxcf,xfd->sxcd", activation, expert_down, preferred_element_type=jnp.float32
    )
    return partial_value.reshape(buffer_shape)


def shards(
    conv_input,
    gate_branch,
    conv_taps,
    narrow_maps,
    wide_maps,
    decay_param,
    decay_shift,
    mixer_out,
    stream,
    norm_gain,
    routes,
    route_weights,
    expert_gate,
    expert_up,
    expert_down,
):
    seq_rows, channels = conv_input.shape
    tap_count = conv_taps.shape[0]
    earlier = shifted(conv_input[seq_rows - tap_count + 1 :], "sp", 1)
    padded = jnp.concatenate([earlier, conv_input], axis=0).astype(jnp.float32)
    convolved = jnp.zeros((seq_rows, channels), jnp.float32)
    for offset in range(tap_count):
        convolved = convolved + padded[offset : offset + seq_rows] * conv_taps[offset]
    convolved = convolved.astype(jnp.bfloat16)
    gate_pre = head_maps(convolved, narrow_maps, wide_maps)
    log_decay = (
        -DECAY_SCALE * jax.nn.sigmoid(gate_pre[0]) * jax.nn.softplus(-decay_param) + decay_shift
    )
    driving = (
        jnp.sqrt(-jnp.expm1(2.0 * log_decay))
        * jax.nn.sigmoid(gate_pre[1])
        * convolved.astype(jnp.float32)
    )
    identity = (jnp.ones((channels,), jnp.float32), jnp.zeros((channels,), jnp.float32))
    totals = jnp.cumsum(log_decay, axis=0)
    summary = jnp.sum(jnp.exp(totals[-1] - totals) * driving, axis=0)
    carried = entering((jnp.exp(totals[-1]), summary), "sp", combine_steps, identity)
    seeded = driving.at[0].add(jnp.exp(log_decay[0]) * carried[1])
    _, recurrent = lax.associative_scan(combine_steps, (jnp.exp(log_decay), seeded), axis=0)
    gated_rows = (recurrent * jax.nn.gelu(gate_branch.astype(jnp.float32))).astype(jnp.bfloat16)
    tp_count = lax.axis_size("tp")
    tok_local = seq_rows // tp_count
    mixer_sum = sum_at_owner(
        jnp.dot(gated_rows, mixer_out, preferred_element_type=jnp.float32).astype(jnp.bfloat16),
        "tp",
        0,
    )
    hidden_f = stream.astype(jnp.float32) + mixer_sum
    hidden = hidden_f.astype(jnp.bfloat16)
    hidden_f = hidden.astype(jnp.float32)
    normed = (
        hidden_f
        * lax.rsqrt(jnp.mean(hidden_f * hidden_f, axis=-1, keepdims=True) + NORM_EPSILON)
        * norm_gain
    ).astype(jnp.bfloat16)
    model_width = normed.shape[1]
    top_count = routes.shape[1]
    expert_total = expert_gate.shape[0] * lax.axis_size("sp")
    capacity = max(2, 2 * tok_local * top_count // expert_total)
    own_index = lax.axis_index("tp")
    assignments = tok_local * top_count
    own_rows = lax.dynamic_slice_in_dim(routes, own_index * tok_local, tok_local, 0)
    own_routes = own_rows.reshape(assignments)
    own_ranks = slot_ranks(own_routes[None, :], expert_total)[0]
    source = jnp.arange(assignments, dtype=jnp.int32) // top_count
    slot_source = (
        jnp.full((expert_total * capacity,), -1, jnp.int32)
        .at[own_routes * capacity + own_ranks]
        .set(source)
    )
    outgoing = take_rows(normed, slot_source).reshape(expert_total, 1, capacity, model_width)
    partial_value = expert_work(
        lax.all_gather(
            lax.all_to_all(outgoing, "sp", split_axis=0, concat_axis=0, tiled=True),
            "tp",
            axis=1,
            tiled=True,
        ),
        expert_gate,
        expert_up,
        expert_down,
    )
    summed = sum_at_owner(partial_value.astype(jnp.bfloat16), "tp", 1).astype(jnp.bfloat16)
    returned = lax.all_to_all(summed, "sp", split_axis=0, concat_axis=0, tiled=True)
    own_slots = own_routes * capacity + own_ranks
    picked = returned.reshape(expert_total * capacity, model_width)[own_slots]
    own_weights = lax.dynamic_slice_in_dim(route_weights, own_index * tok_local, tok_local, 0)
    combined = jnp.sum(
        picked.reshape(tok_local, top_count, model_width).astype(jnp.float32)
        * own_weights[:, :, None],
        axis=1,
    )
    return (hidden_f + combined).astype(jnp.bfloat16)


def solution(mesh):
    placed = (
        P("sp", "tp"),
        P("sp", "tp"),
        P(None, "tp"),
        P(None, "tp", None, None),
        P(None, "tp", None, None),
        P("tp"),
        P("sp", "tp"),
        P("tp", None),
        P(("sp", "tp"), None),
        P(),
        P("sp", None),
        P("sp", None),
        P("sp", None, "tp"),
        P("sp", None, "tp"),
        P("sp", "tp", None),
    )
    return jax.shard_map(
        shards, mesh=mesh, in_specs=placed, out_specs=P(("sp", "tp"), None), check_vma=False
    )
```

profile of v0, /device:TPU:1, one launch (start us, length us, event | category | flops | bytes accessed | tf_op | source)
XLA Modules:
  0.0 514.0 jit_solution(14866498710976884430)
XLA Ops:
  7.4 4.6 collective-permute-start
  20.8 2.1 fusion.75
  25.5 1.5 multiply_reduce_fusion.1
  27.8 11.7 %all-to-all-start = ((f32[64,2,512]{2,1,0:T(2,128)}), f32[64,2,512]{2,1,0:T(2,128)}, u32[]{:S(2)}, u32[]{:S(2)}) async-start(f32[64,2,512]{2,1,0:T(2,128)} %broadcast_in_dim.51), calls=%async_computation | async-start | bytes 524288 | tf_op jit(solution)/shard_map/all_to_all | solution.py:20
  40.5 2.6 slice.380
  43.1 2.5 slice.384
  45.6 1.9 slice.379
  47.5 5.0 all-to-all-done
  54.5 1.5 slice.355
  56.0 1.5 slice.356
  69.1 1.8 fusion.80
  72.2 1.5 slice.392
  73.7 1.5 slice.396
  75.2 1.6 fusion.81
  112.7 1.5 slice.430
  115.5 1.5 slice.391
  130.6 3.5 convolution_convert_fusion
  134.1 4.2 all-to-all-start.1
  140.0 12.9 %all-to-all-done.1 = bf16[4,64,2048]{2,1,0:T(8,128)(2,1)S(1)} async-done(((bf16[4,64,2048]{2,1,0:T(8,128)(2,1)}), bf16[4,64,2048]{2,1,0:T(8,128)(2,1)S(1)}, u32[]{:S(2)}, u32[]{:S(2)}) %all-to-all-start.1) | async-done | bytes 1048608 | tf_op jit(solution)/shard_map/all_to_all | solution.py:70
  154.3 3.3 gather_fusion
  157.6 1.8 bitcast_select_fusion
  159.4 55.9 %all_to_all.25 = bf16[64,1,8,2048]{3,2,1,0:T(8,128)(2,1)} all-to-all(bf16[64,1,8,2048]{3,2,1,0:T(8,128)(2,1)S(1)} %bitcast_select_fusion), channel_id=1, replica_groups=mesh['sp'=64,'tp'=4] {'sp'}, dimensions={0} | all-to-all | bytes 4194304 | tf_op jit(solution)/shard_map/all_to_all | solution.py:209
  215.4 81.3 %all-gather.2.cloned.1.call-done = bf16[64,4,8,2048]{3,2,1,0:T(8,128)(2,1)} async-done(((bf16[64,1,8,2048]{3,2,1,0:T(8,128)(2,1)}), bf16[64,4,8,2048]{3,2,1,0:T(8,128)(2,1)}) %all-gather.2.cloned.1.call-update) | async-done | bytes 8388624 | tf_op jit(solution)/shard_map/all_gather | solution.py:208
  296.7 10.4 %fusion = f32[64,32,512]{2,1,0:T(8,128)} fusion(bf16[64,4,8,2048]{3,2,1,0:T(8,128)(2,1)} %all-gather.2.cloned.1.call-done, bf16[1,2048,512]{2,1,0:T(8,128)(2,1)} %param.29), kind=kOutput, calls=%fused_computation.3 | convolution fusion | flops 4294967296 | bytes 14680064 | tf_op jit(solution)/shard_map/sxcd,xdf->sxcf/dot_general | solution.py:124
  307.2 15.2 %convert_bitcast_fusion = bf16[64,4,1,8,2048]{4,3,1,0,2:T(8,128)(2,1)} fusion(bf16[1,512,2048]{2,1,0:T(8,128)(2,1)S(1)} %copy-done, f32[64,32,512]{2,1,0:T(8,128)} %fusion, bf16[64,4,8,2048]{3,2,1,0:T(8,128)(2,1)} %all-gather.2.cloned.1.call-done, bf16[1,2048,512]{2,1,0:T(8,128)(2,1)} %param.30), kind=kOutput, calls=%fused_computation.8 | convolution fusion | flops 8604614656 | bytes 25165824 | tf_op jit(solution)/shard_map/sxcf,xfd->sxcd/dot_general | solution.py:129
  322.4 8.3 %copy.78 = bf16[64,4,1,8,2048]{4,3,0,2,1:T(8,128)(2,1)} copy(bf16[64,4,1,8,2048]{4,3,1,0,2:T(8,128)(2,1)} %convert_bitcast_fusion) | data formatting | bytes 16777216 | tf_op jit(solution)/shard_map/convert_element_type | solution.py:218
  330.7 100.3 %all_to_all.26 = bf16[4,64,1,8,2048]{4,3,1,2,0:T(8,128)(2,1)} all-to-all(bf16[4,64,1,8,2048]{4,3,1,2,0:T(8,128)(2,1)} %bitcast.119), channel_id=1, replica_groups=mesh['sp'=64,'tp'=4] {'tp'}, dimensions={0} | all-to-all | bytes 16777216 | tf_op jit(solution)/shard_map/all_to_all | solution.py:70
  430.9 7.2 %reduce_sum.63 = bf16[64,8,2048]{2,1,0:T(8,128)(2,1)} reduce(bf16[4,64,1,8,2048]{4,3,1,2,0:T(8,128)(2,1)} %all_to_all.26, bf16[]{:T(256)} %constant.108.clone.1), dimensions={0,2}, to_apply=%region_9.10 | reduce | flops 3145728 | bytes 10485762 | tf_op jit(solution)/shard_map/reduce_sum | solution.py:71
  438.1 12.3 %all-to-all-start.4 = ((bf16[64,1,8,2048]{3,2,1,0:T(8,128)(2,1)}), bf16[64,1,8,2048]{3,2,1,0:T(8,128)(2,1)S(1)}, u32[]{:S(2)}, u32[]{:S(2)}) async-start(bf16[64,1,8,2048]{3,2,1,0:T(8,128)(2,1)} %bitcast.120), calls=%async_computation.4 | async-start | bytes 4194304 | tf_op jit(solution)/shard_map/all_to_all | solution.py:219
  450.6 49.5 %all-to-all-done.4 = bf16[64,1,8,2048]{3,2,1,0:T(8,128)(2,1)S(1)} async-done(((bf16[64,1,8,2048]{3,2,1,0:T(8,128)(2,1)}), bf16[64,1,8,2048]{3,2,1,0:T(8,128)(2,1)S(1)}, u32[]{:S(2)}, u32[]{:S(2)}) %all-to-all-start.4) | async-done | bytes 2097184 | tf_op jit(solution)/shard_map/all_to_all | solution.py:219
  501.5 1.7 reshape.348
  503.2 3.2 multiply_reduce_fusion
  (197 shorter events, 84.7 us)
Async XLA Ops:
  6.5 300.7 %copy-start = (bf16[1,512,2048]{2,1,0:T(8,128)(2,1)S(1)}, bf16[1,512,2048]{2,1,0:T(8,128)(2,1)}, u32[]{:S(2)}) copy-start(bf16[1,512,2048]{2,1,0:T(8,128)(2,1)} %param.31) | copy-start | bytes 6291460
  7.4 8.6 %collective-permute-start = (bf16[3,512]{1,0:T(4,128)(2,1)S(1)}, bf16[3,512]{1,0:T(4,128)(2,1)S(1)}, u32[]{:S(2)}, u32[]{:S(2)}) collective-permute-start(bf16[3,512]{1,0:T(4,128)(2,1)S(1)} %slice.336), channel_id=1, source_target_pairs={{0,4},{4,8},{8,12},{12,16},{16,20},{20,24},{24,28},{28,32},{32,36}... | collective-permute-start | bytes 9224 | tf_op jit(solution)/shard_map/ppermute | solution.py:15
  13.5 3.9 copy-start.8
  20.0 0.8 copy-start.2
  23.3 0.8 copy-start.6
  24.2 1.3 copy-start.3
  24.2 1.4 copy-start.4
  27.8 24.7 %all-to-all-start = ((f32[64,2,512]{2,1,0:T(2,128)}), f32[64,2,512]{2,1,0:T(2,128)}, u32[]{:S(2)}, u32[]{:S(2)}) async-start(f32[64,2,512]{2,1,0:T(2,128)} %broadcast_in_dim.51), calls=%async_computation | async-start | bytes 524288 | tf_op jit(solution)/shard_map/all_to_all | solution.py:20
  40.5 21.7 %copy-start.5 = (f32[256,512]{1,0:T(8,128)S(1)}, f32[256,512]{1,0:T(8,128)}, u32[]{:S(2)}) copy-start(f32[256,512]{1,0:T(8,128)} %get-tuple-element.24) | copy-start | bytes 1572868
  62.2 1.5 copy-start.9
  118.4 8.1 %copy-start.7 = (f32[31,512]{1,0:T(8,128)S(1)}, f32[31,512]{1,0:T(8,128)}, u32[]{:S(2)}) copy-start(f32[31,512]{1,0:T(8,128)} %slice.391) | copy-start | bytes 190468
  119.2 8.1 %copy-start.13 = (f32[1,512]{1,0:T(1,128)S(1)}, f32[1,512]{1,0:T(1,128)}, u32[]{:S(2)}) copy-start(f32[1,512]{1,0:T(1,128)} %slice.463) | copy-start | bytes 6148
  119.2 8.3 %copy-start.12 = (f32[1,512]{1,0:T(1,128)S(1)}, f32[1,512]{1,0:T(1,128)}, u32[]{:S(2)}) copy-start(f32[1,512]{1,0:T(1,128)} %slice.462) | copy-start | bytes 6148
  127.5 3.0 copy-start.10
  134.0 4.2 copy-start.14
  134.0 4.4 copy-start.15
  134.1 20.1 %copy-start.11 = (f32[2048]{0:T(1024)S(1)}, f32[2048]{0:T(1024)}, u32[]{:S(2)}) copy-start(f32[2048]{0:T(1024)} %param.26) | copy-start | bytes 24580
  134.1 18.8 %all-to-all-start.1 = ((bf16[4,64,2048]{2,1,0:T(8,128)(2,1)}), bf16[4,64,2048]{2,1,0:T(8,128)(2,1)S(1)}, u32[]{:S(2)}, u32[]{:S(2)}) async-start(bf16[4,64,2048]{2,1,0:T(8,128)(2,1)} %bitcast.27), calls=%async_computation.1 | async-start | bytes 2097152 | tf_op jit(solution)/shard_map/all_to_all | solution.py:70
  138.2 158.5 %all-gather.2.cloned.1.call-start = ((), (), s32[]{:S(2)}) async-start(), calls=%async_computation.5 | async-start | bytes 10485760 | tf_op jit(solution)/shard_map/all_gather | solution.py:208
  438.1 12.3 %copy-start.16 = (f32[256,4]{0,1:T(4,128)S(1)}, f32[256,4]{0,1:T(4,128)}, u32[]{:S(2)}) copy-start(f32[256,4]{0,1:T(4,128)} %param.28) | copy-start | bytes 12292
  438.1 62.0 %all-to-all-start.4 = ((bf16[64,1,8,2048]{3,2,1,0:T(8,128)(2,1)}), bf16[64,1,8,2048]{3,2,1,0:T(8,128)(2,1)S(1)}, u32[]{:S(2)}, u32[]{:S(2)}) async-start(bf16[64,1,8,2048]{3,2,1,0:T(8,128)(2,1)} %bitcast.120), calls=%async_computation.4 | async-start | bytes 4194304 | tf_op jit(solution)/shard_map/all_to_all | solution.py:219
  501.5 5.7 %copy-start.1 = (bf16[1,512,2048]{2,1,0:T(8,128)(2,1)S(1)}, bf16[1,512,2048]{2,1,0:T(8,128)(2,1)}, u32[]{:S(2)}) copy-start(bf16[1,512,2048]{2,1,0:T(8,128)(2,1)} %param.31) | copy-start | bytes 6291460
Sparse Core Ops, SparseCore 0:
  215.5 81.1 all-gather.1
where the time goes:
time: 518 us; the launch traced here: 514 us
  blocking collectives  156 us (30%)
  waiting for transfers between devices  149 us (29%)
  local copies, waits for them, and re-layouts  84.9 us (16%)
  other arithmetic  46.9 us (9%)
  starting transfers between devices  32.7 us (6%)
  matrix products  30.6 us (6%)
  between operations  14 us (3%)
    all_to_all x1, blocking collectives, sum_at_owner(): blocks = lax.all_to_all(cut_along(x, dim, length), axis, 0, 0, tiled=True)  100 us
    all_gather x1, waiting for transfers between devices, shards(): lax.all_gather(lax.all_to_all(outgoing, 'sp', split_axis=0, concat_axis=0...  81.3 us
    all_to_all x1, blocking collectives, shards(): lax.all_to_all(outgoing, 'sp', split_axis=0, concat_axis=0, tiled=True)  55.9 us
    slice x45, local copies, waits for them, and re-layouts, shards(): lax.associative_scan(combine_steps, (jnp.exp(log_decay), seeded), axis=0)  53.1 us
    all_to_all x1, waiting for transfers between devices, shards(): lax.all_to_all(summed, 'sp', split_axis=0, concat_axis=0, tiled=True)  49.5 us
    dot_general x1, matrix products, expert_work(): jnp.einsum('sxcf,xfd->sxcd', activation, expert_down, preferred_element_t...  15.2 us
    all_to_all x1, waiting for transfers between devices, sum_at_owner(): blocks = lax.all_to_all(cut_along(x, dim, length), axis, 0, 0, tiled=True)  12.9 us
    all_to_all x1, starting transfers between devices, shards(): lax.all_to_all(summed, 'sp', split_axis=0, concat_axis=0, tiled=True)  12.3 us
  transfers between devices with their start and end apart: 5, of which 4 were waited for; matrix products, arithmetic and copies ran while one was open for 3% of the time, Pallas kernels for 0%

commit v1 on v0

v1 whole, which is shorter than its diff:
```python
import jax
import jax.numpy as jnp
from jax import lax
from jax.experimental import pallas as pl
from jax.experimental.pallas import tpu as pltpu
from jax.sharding import PartitionSpec as P

NORM_EPSILON = 1e-06
CLAMP_LIMIT = 7.0
GATE_SLOPE = 1.702
DECAY_SCALE = 8.0
PLANE = 8
MESH = pl.DeviceIdType.MESH
F32 = jnp.float32
BF16 = jnp.bfloat16


def one_minus_exp(x):
    series = 1.0 + x * (1.0 / 9.0)
    for k in range(8, 1, -1):
        series = 1.0 + x * (1.0 / k) * series
    return jnp.where(x > -0.5, -x * series, 1.0 - jnp.exp(x))


def softplus_neg(p):
    u = jnp.exp(-p)
    series = u * (1.0 - u * (1.0 / 2 - u * (1.0 / 3 - u * (1.0 / 4 - u * (1.0 / 5)))))
    return jnp.where(u < 0.02, series, jnp.log(1.0 + u))


def gelu(x):
    inner = 0.7978845608028654 * (x + 0.044715 * x * x * x)
    return 0.5 * x * (1.0 + jnp.tanh(inner))


def sigmoid(x):
    return jax.nn.sigmoid(x)


def mixer_kernel(
    sp_count,
    tp_count,
    conv_ref,
    gate_ref,
    taps_ref,
    narrow_ref,
    wide_ref,
    decay_ref,
    shift_ref,
    mixer_ref,
    stream_ref,
    gain_ref,
    hidden_ref,
    normed_ref,
    halo,
    padded,
    gates,
    cum,
    local,
    comm_a,
    comm_b,
    gated,
    part,
    relay,
    final,
    halo_sems,
    a_sems,
    b_sems,
    r_sems,
):
    s = lax.axis_index("sp")
    x = lax.axis_index("tp")
    z, p = s // PLANE, s % PLANE
    z_count = sp_count // PLANE
    rows, channels = conv_ref.shape
    own = rows // tp_count
    half = own // 2

    def at_sp(i):
        return {"sp": i, "tp": x}

    def at_tp(i):
        return {"sp": s, "tp": i}

    right, left = lax.rem(x + 1, tp_count), lax.rem(x + tp_count - 1, tp_count)
    opposite = lax.rem(x + 2, tp_count)
    after, before = lax.rem(s + 1, sp_count), lax.rem(s + sp_count - 1, sp_count)
    barrier = pltpu.get_barrier_semaphore()
    partners = [at_sp(after), at_sp(before), at_tp(right), at_tp(left)]
    plane = [at_sp(z * PLANE + lax.rem(p + r, PLANE)) for r in range(1, PLANE)]
    column = [at_sp(lax.rem(z + r, z_count) * PLANE + p) for r in range(1, z_count)]
    partners += plane + column
    for to in partners:
        pl.semaphore_signal(barrier, inc=1, device_id=to, device_id_type=MESH)
    pl.semaphore_wait(barrier, len(partners))

    def copy(src, dst, sems, i, to):
        return pltpu.make_async_remote_copy(
            src_ref=src,
            dst_ref=dst,
            send_sem=sems.at[0, i],
            recv_sem=sems.at[1, i],
            device_id=to,
            device_id_type=MESH,
        )

    halo_copy = copy(conv_ref.at[pl.ds(rows - 16, 16)], halo, halo_sems, 0, at_sp(after))
    halo_copy.start()
    padded[pl.ds(16, rows), :] = conv_ref[...].astype(F32)
    halo_copy.wait()
    earlier = halo[...].astype(F32)
    padded[pl.ds(0, 16), :] = jnp.where(s == 0, jnp.zeros_like(earlier), earlier)
    taps = taps_ref[...]
    convolved = padded[pl.ds(13, rows), :] * taps[0:1]
    for k in range(1, 4):
        convolved = convolved + padded[pl.ds(13 + k, rows), :] * taps[k : k + 1]
    convolved = convolved.astype(BF16)
    width = narrow_ref.shape[3]
    heads = narrow_ref.shape[1]
    for m in range(2):
        for h in range(heads):
            cut = slice(h * width, (h + 1) * width)
            gates[m, :, cut] = jnp.dot(
                convolved[:, cut], narrow_ref[m, h], preferred_element_type=F32
            )
        gates[m, :, heads * width :] = jnp.dot(
            convolved[:, heads * width :], wide_ref[m, 0], preferred_element_type=F32
        )
    rate = softplus_neg(decay_ref[...])
    row = lax.broadcasted_iota(jnp.int32, (rows, 128), 0)
    for j in range(channels // 128):
        cut = slice(j * 128, (j + 1) * 128)
        log_decay = -DECAY_SCALE * sigmoid(gates[0, :, cut]) * rate[:, cut] + shift_ref[:, cut]
        b = (
            jnp.sqrt(one_minus_exp(2.0 * log_decay))
            * sigmoid(gates[1, :, cut])
            * convolved[:, cut].astype(F32)
        )
        a = jnp.exp(log_decay)
        step = 1
        while step < rows:
            if step < 8:
                a_back = jnp.where(row >= step, pltpu.roll(a, step, 0), 1.0)
                b_back = jnp.where(row >= step, pltpu.roll(b, step, 0), 0.0)
            else:
                a_back = jnp.concatenate([jnp.ones((step, 128), F32), a[: rows - step]], axis=0)
                b_back = jnp.concatenate([jnp.zeros((step, 128), F32), b[: rows - step]], axis=0)
            b = a * b_back + b
            a = a * a_back
            step *= 2
        cum[:, cut] = a
        local[:, cut] = b
        comm_a[p, pl.ds(j, 1), :] = a[rows - 1 :]
        comm_a[p, pl.ds(4 + j, 1), :] = b[rows - 1 :]

    sends = [
        copy(comm_a.at[p], comm_a.at[p], a_sems, r, to) for r, to in enumerate(plane)
    ]
    for c in sends:
        c.start()
    for j in range(channels // 128):
        cut = slice(j * 128, (j + 1) * 128)
        gates[0, :, cut] = gelu(gate_ref[:, cut].astype(F32))
    for c in sends:
        c.wait()
    a_before, b_before = jnp.ones((4, 128), F32), jnp.zeros((4, 128), F32)
    a_all, b_all = a_before, b_before
    for q in range(PLANE):
        a, b = comm_a[q, 0:4, :], comm_a[q, 4:8, :]
        inside = q < p
        b_before = jnp.where(inside, a * b_before + b, b_before)
        a_before = jnp.where(inside, a * a_before, a_before)
        b_all = a * b_all + b
        a_all = a * a_all
    comm_b[z, 0:4, :] = a_all
    comm_b[z, 4:8, :] = b_all
    sends = [
        copy(comm_b.at[z], comm_b.at[z], b_sems, r, to) for r, to in enumerate(column)
    ]
    for c in sends:
        c.start()
    for c in sends:
        c.wait()
    state = jnp.zeros((4, 128), F32)
    for q in range(z_count):
        state = jnp.where(q < z, comm_b[q, 0:4, :] * state + comm_b[q, 4:8, :], state)
    state = a_before * state + b_before
    for j in range(channels // 128):
        cut = slice(j * 128, (j + 1) * 128)
        recurrent = local[:, cut] + cum[:, cut] * state[j : j + 1, :]
        gated[:, cut] = (recurrent * gates[0, :, cut]).astype(BF16)
    features = mixer_ref.shape[1]
    for j in range(features // 512):
        cut = slice(j * 512, (j + 1) * 512)
        part[:, cut] = jnp.dot(
            gated[...], mixer_ref[:, cut], preferred_element_type=F32
        ).astype(BF16)

    def rows_of(o, first, count):
        return pl.ds(pl.multiple_of(o * own + first, half), count)

    to_right, to_left = at_tp(right), at_tp(left)
    out = [
        copy(part.at[rows_of(opposite, 0, half)], relay.at[0], r_sems, 0, to_right),
        copy(part.at[rows_of(opposite, half, half)], relay.at[1], r_sems, 1, to_left),
        copy(
            part.at[rows_of(right, half, half)],
            final.at[0, pl.ds(half, half)],
            r_sems,
            2,
            to_right,
        ),
        copy(
            part.at[rows_of(left, 0, half)], final.at[1, pl.ds(0, half)], r_sems, 3, to_left
        ),
        copy(
            part.at[rows_of(right, 0, half)], final.at[0, pl.ds(0, half)], r_sems, 4, to_right
        ),
        copy(
            part.at[rows_of(left, half, half)],
            final.at[1, pl.ds(half, half)],
            r_sems,
            5,
            to_left,
        ),
    ]
    for c in out[:4]:
        c.start()
    for side, (o, first) in enumerate(((right, 0), (left, half))):
        out[side].wait_recv()
        where = rows_of(o, first, half)
        part[where, :] = (part[where, :].astype(F32) + relay[side].astype(F32)).astype(BF16)
        out[4 + side].start()
    base = stream_ref[...].astype(F32) + part[rows_of(x, 0, own), :].astype(F32)
    for c in out[2:]:
        c.wait_recv()
    hidden = (base + (final[0].astype(F32) + final[1].astype(F32))).astype(BF16)
    hidden_ref[...] = hidden
    hidden_f = hidden.astype(F32)
    mean = jnp.mean(hidden_f * hidden_f, axis=-1, keepdims=True)
    normed_ref[...] = (hidden_f * lax.rsqrt(mean + NORM_EPSILON) * gain_ref[...]).astype(BF16)
    for c in out:
        c.wait_send()


def mixer_stage(
    sp_count,
    tp_count,
    conv_input,
    gate_branch,
    conv_taps,
    narrow_maps,
    wide_maps,
    decay_param,
    decay_shift,
    mixer_out,
    stream,
    norm_gain,
):
    import functools

    rows, channels = conv_input.shape
    own, features = stream.shape
    vmem = pl.BlockSpec(memory_space=pltpu.VMEM)
    dma = pltpu.SemaphoreType.DMA
    return pl.pallas_call(
        functools.partial(mixer_kernel, sp_count, tp_count),
        out_shape=[jax.ShapeDtypeStruct((own, features), BF16)] * 2,
        in_specs=[vmem] * 10,
        out_specs=[vmem] * 2,
        scratch_shapes=[
            pltpu.VMEM((16, channels), BF16),
            pltpu.VMEM((rows + 16, channels), F32),
            pltpu.VMEM((2, rows, channels), F32),
            pltpu.VMEM((rows, channels), F32),
            pltpu.VMEM((rows, channels), F32),
            pltpu.VMEM((PLANE, 8, 128), F32),
            pltpu.VMEM((sp_count // PLANE, 8, 128), F32),
            pltpu.VMEM((rows, channels), BF16),
            pltpu.VMEM((rows, features), BF16),
            pltpu.VMEM((2, own // 2, features), BF16),
            pltpu.VMEM((2, own, features), BF16),
            dma((2, 1)),
            dma((2, PLANE - 1)),
            dma((2, sp_count // PLANE - 1)),
            dma((2, 6)),
        ],
        compiler_params=pltpu.CompilerParams(collective_id=0, has_side_effects=True),
    )(
        conv_input,
        gate_branch,
        conv_taps,
        narrow_maps,
        wide_maps,
        decay_param.reshape(1, -1),
        decay_shift,
        mixer_out,
        stream,
        norm_gain.reshape(1, -1),
    )


def cut_along(x, dim, length):
    lengths = x.shape
    blocks = x.reshape(*lengths[:dim], length, lengths[dim] // length, *lengths[dim + 1 :])
    return jnp.moveaxis(blocks, dim, 0)


def sum_at_owner(x, axis, dim):
    length = lax.axis_size(axis)
    blocks = lax.all_to_all(cut_along(x, dim, length), axis, 0, 0, tiled=True)
    return jnp.sum(blocks.astype(jnp.float32), axis=0)


def clamp_units(gate_pre, up_pre):
    clamped = jnp.minimum(gate_pre, CLAMP_LIMIT)
    upper = jnp.clip(up_pre, -CLAMP_LIMIT, CLAMP_LIMIT)
    return (upper + 1.0) * clamped * jax.nn.sigmoid(GATE_SLOPE * clamped)


def slot_ranks(flat_routes, expert_total):
    onehot = (
        flat_routes[:, :, None] == jnp.arange(expert_total, dtype=jnp.int32)[None, None, :]
    ).astype(jnp.int32)
    return jnp.sum(jnp.cumsum(onehot, axis=1) * onehot, axis=2) - 1


def take_rows(source_rows, slot_source):
    filled = slot_source >= 0
    picked = source_rows[jnp.maximum(slot_source, 0)]
    return jnp.where(filled[:, None], picked, jnp.zeros_like(picked))


def expert_work(arrived, expert_gate, expert_up, expert_down):
    local_experts = expert_gate.shape[0]
    buffer_shape = arrived.shape
    grouped = arrived.reshape(
        buffer_shape[0] // local_experts,
        local_experts,
        buffer_shape[1] * buffer_shape[2],
        buffer_shape[3],
    )
    gate_pre = jnp.einsum(
        "sxcd,xdf->sxcf", grouped, expert_gate, preferred_element_type=jnp.float32
    )
    up_pre = jnp.einsum("sxcd,xdf->sxcf", grouped, expert_up, preferred_element_type=jnp.float32)
    activation = clamp_units(gate_pre, up_pre).astype(jnp.bfloat16)
    partial_value = jnp.einsum(
        "sxcf,xfd->sxcd", activation, expert_down, preferred_element_type=jnp.float32
    )
    return partial_value.reshape(buffer_shape)


def shards(
    conv_input,
    gate_branch,
    conv_taps,
    narrow_maps,
    wide_maps,
    decay_param,
    decay_shift,
    mixer_out,
    stream,
    norm_gain,
    routes,
    route_weights,
    expert_gate,
    expert_up,
    expert_down,
):
    tp_count = lax.axis_size("tp")
    tok_local = stream.shape[0]
    hidden, normed = mixer_stage(
        lax.axis_size("sp"), tp_count, conv_input, gate_branch, conv_taps, narrow_maps,
        wide_maps, decay_param, decay_shift, mixer_out, stream, norm_gain,
    )
    hidden_f = hidden.astype(jnp.float32)
    model_width = normed.shape[1]
    top_count = routes.shape[1]
    expert_total = expert_gate.shape[0] * lax.axis_size("sp")
    capacity = max(2, 2 * tok_local * top_count // expert_total)
    own_index = lax.axis_index("tp")
    assignments = tok_local * top_count
    own_rows = lax.dynamic_slice_in_dim(routes, own_index * tok_local, tok_local, 0)
    own_routes = own_rows.reshape(assignments)
    own_ranks = slot_ranks(own_routes[None, :], expert_total)[0]
    source = jnp.arange(assignments, dtype=jnp.int32) // top_count
    slot_source = (
        jnp.full((expert_total * capacity,), -1, jnp.int32)
        .at[own_routes * capacity + own_ranks]
        .set(source)
    )
    outgoing = take_rows(normed, slot_source).reshape(expert_total, 1, capacity, model_width)
    partial_value = expert_work(
        lax.all_gather(
            lax.all_to_all(outgoing, "sp", split_axis=0, concat_axis=0, tiled=True),
            "tp",
            axis=1,
            tiled=True,
        ),
        expert_gate,
        expert_up,
        expert_down,
    )
    summed = sum_at_owner(partial_value.astype(jnp.bfloat16), "tp", 1).astype(jnp.bfloat16)
    returned = lax.all_to_all(summed, "sp", split_axis=0, concat_axis=0, tiled=True)
    own_slots = own_routes * capacity + own_ranks
    picked = returned.reshape(expert_total * capacity, model_width)[own_slots]
    own_weights = lax.dynamic_slice_in_dim(route_weights, own_index * tok_local, tok_local, 0)
    combined = jnp.sum(
        picked.reshape(tok_local, top_count, model_width).astype(jnp.float32)
        * own_weights[:, :, None],
        axis=1,
    )
    return (hidden_f + combined).astype(jnp.bfloat16)


def solution(mesh):
    placed = (
        P("sp", "tp"),
        P("sp", "tp"),
        P(None, "tp"),
        P(None, "tp", None, None),
        P(None, "tp", None, None),
        P("tp"),
        P("sp", "tp"),
        P("tp", None),
        P(("sp", "tp"), None),
        P(),
        P("sp", None),
        P("sp", None),
        P("sp", None, "tp"),
        P("sp", None, "tp"),
        P("sp", "tp", None),
    )
    return jax.shard_map(
        shards, mesh=mesh, in_specs=placed, out_specs=P(("sp", "tp"), None), check_vma=False
    )
```

time: 518 us -> 416 us (0.80)
  local copies, waits for them, and re-layouts: 84.9 us -> 23 us
  Pallas kernels: 0 us -> 34.8 us
  other arithmetic: 46.9 us -> 14.7 us
  starting transfers between devices: 32.7 us -> 12.3 us
  waiting for transfers between devices: 149 us -> 132 us
    slice x70 -> x1, local copies, waits for them, and re-layouts: 62 us -> 0.18 us  [the longest x45 53.1 us: shards(): lax.associative_scan(combine_steps, (jnp.exp(log_decay), seeded), axis=0)]
    pallas_call x0 -> x1, Pallas kernels: none -> 34.8 us  [mixer_stage(): pl.pallas_call(functools.partial(mixer_kernel, sp_count, tp_count), out_s...]
    all_to_all x2 -> x0, waiting for transfers between devices: 17.9 us -> none  [the longest x1 12.9 us: sum_at_owner(): blocks = lax.all_to_all(cut_along(x, dim, length), axis, 0, 0, tiled=True)]
    all_to_all x2 -> x0, starting transfers between devices: 15.8 us -> none  [the longest x1 11.7 us: from_everyone(): return lax.all_to_all(copies, axis, split_axis=0, concat_axis=0, tiled=True)]
    mul x11 -> x0, other arithmetic: 11.3 us -> none  [the longest x10 10.6 us: combine_steps(): return (earlier[0] * later[0], later[0] * earlier[1] + later[1])]
    add x16 -> x0, other arithmetic: 6.3 us -> none  [the longest x8 4.89 us: combine_steps(): return (earlier[0] * later[0], later[0] * earlier[1] + later[1])]
  transfers between devices with their start and end apart: 5 -> 2, of which waited for: 4 -> 2; matrix products, arithmetic and copies ran while one was open for 3% -> 0% of each run, Pallas kernels for 0% -> 0%
where the time goes in v1:
time: 416 us; the launch traced here: 415 us
  blocking collectives  160 us (38%)
  waiting for transfers between devices  132 us (32%)
  Pallas kernels  34.8 us (8%)
  matrix products  25.6 us (6%)
  local copies, waits for them, and re-layouts  23 us (6%)
  other arithmetic  14.7 us (4%)
  between operations  13.6 us (3%)
  starting transfers between devices  12.3 us (3%)
    all_to_all x1, blocking collectives, sum_at_owner(): blocks = lax.all_to_all(cut_along(x, dim, length), axis, 0, 0, tiled=True)  100 us
    all_gather x1, waiting for transfers between devices, shards(): lax.all_gather(lax.all_to_all(outgoing, 'sp', split_axis=0, concat_axis=0...  82.1 us
    all_to_all x1, blocking collectives, shards(): lax.all_to_all(outgoing, 'sp', split_axis=0, concat_axis=0, tiled=True)  59.2 us
    all_to_all x1, waiting for transfers between devices, shards(): lax.all_to_all(summed, 'sp', split_axis=0, concat_axis=0, tiled=True)  49.4 us
    pallas_call x1, Pallas kernels, mixer_stage(): pl.pallas_call(functools.partial(mixer_kernel, sp_count, tp_count), out_s...  34.8 us
    dot_general x1, matrix products, expert_work(): jnp.einsum('sxcf,xfd->sxcd', activation, expert_down, preferred_element_t...  15.1 us
    all_to_all x1, starting transfers between devices, shards(): lax.all_to_all(summed, 'sp', split_axis=0, concat_axis=0, tiled=True)  12.3 us
    dot_general x1, matrix products, expert_work(): jnp.einsum('sxcd,xdf->sxcf', grouped, expert_gate, preferred_element_type...  10.4 us
  transfers between devices with their start and end apart: 2, of which 2 were waited for; matrix products, arithmetic and copies ran while one was open for 0% of the time, Pallas kernels for 0%

profile of v1, /device:TPU:1, one launch (start us, length us, event | category | flops | bytes accessed | tf_op | source)
XLA Modules:
  0.0 415.1 jit_solution(17715478740466489476)
XLA Ops:
  6.5 0.9 broadcast_multiply_fusion
  7.4 0.1 copy.26
  7.5 0.1 eq.27
  7.6 0.1 compare_convert_fusion
  7.7 0.6 reduce-window.6
  8.3 0.2 slice_reduce_fusion
  8.5 0.1 copy.28
  8.6 0.1 copy.29
  8.7 0.1 broadcast.158
  8.9 0.1 fusion.13
  9.0 0.1 copy.25
  9.1 0.1 mul.53
  9.2 1.4 scatter_custom_fusion
  10.7 0.1 broadcast_in_dim.25
  10.8 34.8 %shard_map.145 = (bf16[64,2048]{1,0:T(8,128)(2,1)}, bf16[64,2048]{1,0:T(8,128)(2,1)}) custom-call(bf16[256,512]{1,0:T(8,128)(2,1)} %conv_ref.1, bf16[256,512]{1,0:T(8,128)(2,1)} %gate_ref.1, f32[4,512]{1,0:T(4,128)} %taps_ref.1, bf16[2,2,128,128]{3,2,1,0:T(8,128)(2,1)} %narrow_ref.1, bf16[2,1,256,256]{3,2,1,0:T(8,128)(2,1)} %wide_ref.1, f32[1,512]{1,0:T(1,128)} %bitcast.66, ...), custom_call_target="tpu_custom_call" | custom-call | tf_op jit(solution)/shard_map/pallas_call | solution.py:266
  45.6 6.3 %gather_fusion = bf16[512,2048]{1,0:T(8,128)(2,1)} fusion(bf16[64,2048]{1,0:T(8,128)(2,1)} %get-tuple-element.8, s32[1024]{0:T(1024)S(1)} %pad_clamp_fusion.1), kind=kCustom, calls=%fused_computation | custom fusion | bytes 4196352 | tf_op jit(solution)/shard_map/gather | solution.py:330
  51.8 1.8 bitcast_select_fusion
  53.6 59.2 %all_to_all.15 = bf16[64,1,8,2048]{3,2,1,0:T(8,128)(2,1)} all-to-all(bf16[64,1,8,2048]{3,2,1,0:T(8,128)(2,1)S(1)} %bitcast_select_fusion), channel_id=1, replica_groups=mesh['sp'=64,'tp'=4] {'sp'}, dimensions={0} | all-to-all | bytes 4194304 | tf_op jit(solution)/shard_map/all_to_all | solution.py:396
  112.9 82.1 %all-gather.2.cloned.1.call-done = bf16[64,4,8,2048]{3,2,1,0:T(8,128)(2,1)} async-done(((bf16[64,1,8,2048]{3,2,1,0:T(8,128)(2,1)}), bf16[64,4,8,2048]{3,2,1,0:T(8,128)(2,1)}) %all-gather.2.cloned.1.call-update) | async-done | bytes 8388624 | tf_op jit(solution)/shard_map/all_gather | solution.py:395
  195.0 10.4 %fusion = f32[64,32,512]{2,1,0:T(8,128)} fusion(bf16[64,4,8,2048]{3,2,1,0:T(8,128)(2,1)} %all-gather.2.cloned.1.call-done, bf16[1,2048,512]{2,1,0:T(8,128)(2,1)} %param.27), kind=kOutput, calls=%fused_computation.3 | convolution fusion | flops 4294967296 | bytes 14680064 | tf_op jit(solution)/shard_map/sxcd,xdf->sxcf/dot_general | solution.py:343
  205.5 15.1 %convert_bitcast_fusion = bf16[64,4,1,8,2048]{4,3,1,0,2:T(8,128)(2,1)} fusion(bf16[1,512,2048]{2,1,0:T(8,128)(2,1)S(1)} %copy-done, f32[64,32,512]{2,1,0:T(8,128)} %fusion, bf16[64,4,8,2048]{3,2,1,0:T(8,128)(2,1)} %all-gather.2.cloned.1.call-done, bf16[1,2048,512]{2,1,0:T(8,128)(2,1)} %param.28), kind=kOutput, calls=%fused_computation.8 | convolution fusion | flops 8604614656 | bytes 25165824 | tf_op jit(solution)/shard_map/sxcf,xfd->sxcd/dot_general | solution.py:348
  220.6 8.3 %copy.34 = bf16[64,4,1,8,2048]{4,3,0,2,1:T(8,128)(2,1)} copy(bf16[64,4,1,8,2048]{4,3,1,0,2:T(8,128)(2,1)} %convert_bitcast_fusion) | data formatting | bytes 16777216 | tf_op jit(solution)/shard_map/convert_element_type | solution.py:405
  228.9 100.3 %all_to_all.16 = bf16[4,64,1,8,2048]{4,3,1,2,0:T(8,128)(2,1)} all-to-all(bf16[4,64,1,8,2048]{4,3,1,2,0:T(8,128)(2,1)} %bitcast.56), channel_id=1, replica_groups=mesh['sp'=64,'tp'=4] {'tp'}, dimensions={0} | all-to-all | bytes 16777216 | tf_op jit(solution)/shard_map/all_to_all | solution.py:311
  329.2 7.2 %reduce_sum.33 = bf16[64,8,2048]{2,1,0:T(8,128)(2,1)} reduce(bf16[4,64,1,8,2048]{4,3,1,2,0:T(8,128)(2,1)} %all_to_all.16, bf16[]{:T(256)} %constant.51.clone.1), dimensions={0,2}, to_apply=%region_4.5 | reduce | flops 3145728 | bytes 10485762 | tf_op jit(solution)/shard_map/reduce_sum | solution.py:312
  336.4 12.3 %all-to-all-start.2 = ((bf16[64,1,8,2048]{3,2,1,0:T(8,128)(2,1)}), bf16[64,1,8,2048]{3,2,1,0:T(8,128)(2,1)}, u32[]{:S(2)}, u32[]{:S(2)}) async-start(bf16[64,1,8,2048]{3,2,1,0:T(8,128)(2,1)} %bitcast.57), calls=%async_computation.2 | async-start | bytes 4194304 | tf_op jit(solution)/shard_map/all_to_all | solution.py:406
  348.7 0.1 constant_dynamic-slice_fusion
  348.8 0.1 copy.32
  348.9 49.4 %all-to-all-done.2 = bf16[64,1,8,2048]{3,2,1,0:T(8,128)(2,1)} async-done(((bf16[64,1,8,2048]{3,2,1,0:T(8,128)(2,1)}), bf16[64,1,8,2048]{3,2,1,0:T(8,128)(2,1)}, u32[]{:S(2)}, u32[]{:S(2)}) %all-to-all-start.2) | async-done | bytes 2097184 | tf_op jit(solution)/shard_map/all_to_all | solution.py:406
  398.3 4.2 %gather_fusion.1 = bf16[256,2048]{1,0:T(8,128)(2,1)S(1)} fusion(bf16[512,2048]{1,0:T(8,128)(2,1)} %bitcast.25, s32[1024]{0:T(1024)S(1)} %pad_clamp_fusion), kind=kCustom, calls=%fused_computation.1 | custom fusion | bytes 2098176 | tf_op jit(solution)/shard_map/gather | solution.py:408
  402.5 1.7 reshape.248
  404.3 3.2 multiply_reduce_fusion
  407.5 0.8 add_convert_fusion
  (18 shorter events, 0.1 us)
Async XLA Ops:
  6.5 198.9 %copy-start = (bf16[1,512,2048]{2,1,0:T(8,128)(2,1)S(1)}, bf16[1,512,2048]{2,1,0:T(8,128)(2,1)}, u32[]{:S(2)}) copy-start(bf16[1,512,2048]{2,1,0:T(8,128)(2,1)} %param.29) | copy-start | bytes 6291460
  6.5 188.5 %all-gather.2.cloned.1.call-start = ((), (), s32[]{:S(2)}) async-start(), calls=%async_computation.3 | async-start | bytes 10485760 | tf_op jit(solution)/shard_map/all_gather | solution.py:395
  336.4 12.3 %copy-start.2 = (f32[256,4]{0,1:T(4,128)S(1)}, f32[256,4]{0,1:T(4,128)}, u32[]{:S(2)}) copy-start(f32[256,4]{0,1:T(4,128)} %param.26) | copy-start | bytes 12292
  336.4 61.9 %all-to-all-start.2 = ((bf16[64,1,8,2048]{3,2,1,0:T(8,128)(2,1)}), bf16[64,1,8,2048]{3,2,1,0:T(8,128)(2,1)}, u32[]{:S(2)}, u32[]{:S(2)}) async-start(bf16[64,1,8,2048]{3,2,1,0:T(8,128)(2,1)} %bitcast.57), calls=%async_computation.2 | async-start | bytes 4194304 | tf_op jit(solution)/shard_map/all_to_all | solution.py:406
  402.5 4.9 %copy-start.1 = (bf16[64,2048]{1,0:T(8,128)(2,1)S(1)}, bf16[64,2048]{1,0:T(8,128)(2,1)}, u32[]{:S(2)}) copy-start(bf16[64,2048]{1,0:T(8,128)(2,1)} %get-tuple-element.7) | copy-start | bytes 786436
Sparse Core Ops, SparseCore 0:
  113.0 81.9 all-gather.1
